TPU v7x, 32 devices: a whole 2x2x4 slice. The times are simulated.
32 devices in a mesh: ep: 8 (over z, x), tp: 4 (over y, core).
Axes of the slice: x: 2, y: 2, z: 4, core: 2. Of those that a mesh axis runs over, the one named last changes fastest.
Arguments:
- stream: bfloat16 [128, 4096], P(None, 'ep'), may hold values from -6.5 to 6.5
- norm_gain: float32 [4096], P('ep'), may hold values from 0.1 to 1.9
- w_query: bfloat16 [4096, 2048], P('ep', 'tp'), may hold values from -0.09375 to 0.09375
- w_key: bfloat16 [4096, 1024], P('ep', 'tp'), may hold values from -0.09375 to 0.09375
- w_value: bfloat16 [4096, 1024], P('ep', 'tp'), may hold values from -0.09375 to 0.09375
- break_offset: float32 [16], P('tp'), may hold values from -10 to -2
- cache_keys: bfloat16 [128, 1024, 8, 128], P('ep', None, 'tp'), may hold values from -6 to 6
- cache_values: bfloat16 [128, 1024, 8, 128], P('ep', None, 'tp'), may hold values from -6 to 6
- lengths: int32 [128], P('ep'), may hold values from 128 to 1024
- w_output: bfloat16 [2048, 4096], P('tp', 'ep'), may hold values from -0.125 to 0.125
- head_gain: float32 [2048], P('tp'), may hold values from 0.1 to 1.9
- ffn_gain: float32 [4096], P('ep'), may hold values from 0.1 to 1.9
- route_experts: int32 [128, 2], replicated, may hold values from 0 to 7, all different within a row; in each aligned block of 128 rows (0 to 127, 128 to 255, ...) at most 64 rows name the same one
- route_weights: float32 [128, 2], replicated, may hold values from 0.1 to 1
- expert_gate: bfloat16 [8, 4096, 1024], P('ep', None, 'tp'), may hold values from -0.09375 to 0.09375
- expert_up: bfloat16 [8, 4096, 1024], P('ep', None, 'tp'), may hold values from -0.09375 to 0.09375
- expert_down: bfloat16 [8, 1024, 4096], P('ep', 'tp'), may hold values from -0.1875 to 0.1875
- dense_gate: bfloat16 [4096, 4096], P('ep', 'tp'), may hold values from -0.09375 to 0.09375
- dense_up: bfloat16 [4096, 4096], P('ep', 'tp'), may hold values from -0.09375 to 0.09375
- dense_down: bfloat16 [4096, 4096], P('tp', 'ep'), may hold values from -0.09375 to 0.09375
- mix_gain: float32 [4096], P('ep'), may hold values from 0.1 to 1.9
Outputs:
- mixed_out: bfloat16 [128, 4096], P(None, 'ep')
- key_rows: bfloat16 [128, 1024], P('ep', 'tp')
- value_rows: bfloat16 [128, 1024], P('ep', 'tp')
Inputs may be any that keep to these rules, and one draw needn't show every extreme that they name: `route_experts`: in the whole batch no expert is named by more than 64 pairs, a bound that some block reaches; the 2 experts of a token differ.
All inputs are finite; a program needn't handle non-finite values.
Results may differ from a plain program's by a relative error of at most 0.025.
Values may be sent and summed in bfloat16 or wider, within the bound.
A program may use at most 64 MiB of HBM per device.

v0:
```python
import jax
import jax.numpy as jnp
from jax import lax
from jax.sharding import PartitionSpec as P

EPSILON = 1e-06


def rms_scale(values, gain_vec, model_width):
    squares = lax.psum(jnp.sum(values * values, axis=1), "ep")
    return values * lax.rsqrt(squares / model_width + EPSILON)[:, None] * gain_vec[None, :]


def to_heads(normed, weights):
    return lax.psum_scatter(
        jnp.dot(normed, weights, preferred_element_type=jnp.float32).astype(jnp.bfloat16),
        "ep",
        scatter_dimension=0,
        tiled=True,
    ).astype(jnp.float32)


def from_heads(values, weights):
    partial_value = jnp.dot(
        lax.all_gather(values, "ep", axis=0, tiled=True),
        weights,
        preferred_element_type=jnp.float32,
    )
    return lax.psum(partial_value.astype(jnp.bfloat16), "tp")


def expert_terms(inputs, gate_w, up_w, down_w):
    gate_val = jnp.einsum("ecd,edf->ecf", inputs, gate_w, preferred_element_type=jnp.float32)
    up_val = jnp.einsum("ecd,edf->ecf", inputs, up_w, preferred_element_type=jnp.float32)
    hidden = (jax.nn.silu(gate_val) * up_val).astype(jnp.bfloat16)
    return jnp.einsum("ecf,efd->ecd", hidden, down_w, preferred_element_type=jnp.float32)


def slot_table(route_experts, experts, capacity):
    chosen = route_experts.reshape(-1)
    onehot = (chosen[:, None] == jnp.arange(experts, dtype=jnp.int32)[None, :]).astype(jnp.int32)
    earlier = jnp.cumsum(onehot, axis=0) - onehot
    rank_in = jnp.sum(earlier * onehot, axis=1)
    slot_ids = chosen * capacity + rank_in
    owners = jnp.arange(chosen.shape[0], dtype=jnp.int32) // route_experts.shape[1]
    filled = (
        jnp.full((experts * capacity,), route_experts.shape[0], jnp.int32).at[slot_ids].set(owners)
    )
    return (slot_ids, filled)


def per_device(
    stream,
    norm_gain,
    w_query,
    w_key,
    w_value,
    break_offset,
    cache_keys,
    cache_values,
    lengths,
    w_output,
    head_gain,
    ffn_gain,
    route_experts,
    route_weights,
    expert_gate,
    expert_up,
    expert_down,
    dense_gate,
    dense_up,
    dense_down,
    mix_gain,
):
    model_width = stream.shape[1] * lax.axis_size("ep")
    block_width = stream.shape[1]
    seq_count = lengths.shape[0]
    kv_local = cache_keys.shape[2]
    head_dim = cache_keys.shape[3]
    heads_local = break_offset.shape[0]
    group_size = heads_local // kv_local
    cache_len = cache_keys.shape[1]
    streamf = stream.astype(jnp.float32)
    normed = rms_scale(streamf, norm_gain, model_width).astype(jnp.bfloat16)
    projected = to_heads(normed, jnp.concatenate([w_query, w_key, w_value], axis=1))
    q_width = w_query.shape[1]
    k_width = w_key.shape[1]
    queries = (
        projected[:, :q_width]
        .astype(jnp.bfloat16)
        .reshape(seq_count, kv_local, group_size, head_dim)
    )
    key_rows = projected[:, q_width : q_width + k_width].astype(jnp.bfloat16)
    value_rows = projected[:, q_width + k_width :].astype(jnp.bfloat16)
    scores = jnp.einsum("skgd,slkd->skgl", queries, cache_keys, preferred_element_type=jnp.float32)
    scores = (
        scores * head_dim ** (-0.5) + break_offset.reshape(kv_local, group_size)[None, :, :, None]
    )
    in_cache = (jnp.arange(cache_len, dtype=jnp.int32)[None, :] < lengths[:, None])[
        :, None, None, :
    ]
    failed = jnp.where(in_cache, jax.nn.log_sigmoid(-scores), 0.0)
    later_sum = lax.cumsum(failed, axis=3, reverse=True) - failed
    weights = jnp.where(in_cache, jnp.exp(jax.nn.log_sigmoid(scores) + later_sum), 0.0).astype(
        jnp.bfloat16
    )
    attended = jnp.einsum(
        "skgl,slkd->skgd", weights, cache_values, preferred_element_type=jnp.float32
    )
    gains = head_gain.reshape(kv_local, group_size, head_dim)[None]
    normalized = (
        attended * lax.rsqrt(jnp.mean(attended * attended, axis=3, keepdims=True) + EPSILON) * gains
    )
    head_out = normalized.astype(jnp.bfloat16).reshape(seq_count, heads_local * head_dim)
    attn_out = from_heads(head_out, w_output)
    residual = streamf + attn_out.astype(jnp.float32)
    normed_ffn = rms_scale(residual, ffn_gain, model_width).astype(jnp.bfloat16)
    dense_width = dense_gate.shape[1]
    gate_up = to_heads(normed_ffn, jnp.concatenate([dense_gate, dense_up], axis=1))
    dense_hidden = (jax.nn.silu(gate_up[:, :dense_width]) * gate_up[:, dense_width:]).astype(
        jnp.bfloat16
    )
    dense_out = from_heads(dense_hidden, dense_down)
    experts = expert_gate.shape[0] * lax.axis_size("ep")
    capacity = 2 * seq_count * route_experts.shape[1] // expert_gate.shape[0]
    slot_ids, filled = slot_table(route_experts, experts, capacity)
    padded = jnp.concatenate([normed_ffn, jnp.zeros((1, block_width), jnp.bfloat16)], axis=0)
    outgoing = padded[filled].reshape(experts, capacity, block_width)
    slot_share = capacity // lax.axis_size("tp")
    own_slots = lax.dynamic_slice_in_dim(outgoing, lax.axis_index("tp") * slot_share, slot_share, 1)
    arrived = lax.all_to_all(own_slots, "ep", split_axis=0, concat_axis=2, tiled=True)
    gathered = lax.all_gather(arrived, "tp", axis=1, tiled=True)
    partial_value = expert_terms(gathered, expert_gate, expert_up, expert_down)
    summed = lax.psum_scatter(
        partial_value.astype(jnp.bfloat16), "tp", scatter_dimension=1, tiled=True
    )
    came_back = lax.all_to_all(summed, "ep", split_axis=2, concat_axis=0, tiled=True)
    returned = lax.all_gather(came_back, "tp", axis=1, tiled=True)
    picked = returned.reshape(experts * capacity, block_width)[slot_ids]
    picked = picked.reshape(route_experts.shape[0], route_experts.shape[1], block_width).astype(
        jnp.float32
    )
    shares = route_weights / jnp.sum(route_weights, axis=1, keepdims=True)
    moe_out = jnp.sum(picked * shares[:, :, None], axis=1)
    mixed_out = (residual + moe_out + mix_gain[None, :] * dense_out.astype(jnp.float32)).astype(
        jnp.bfloat16
    )
    return (mixed_out, key_rows, value_rows)


def solution(mesh):
    in_specs = (
        P(None, "ep"),
        P("ep"),
        P("ep", "tp"),
        P("ep", "tp"),
        P("ep", "tp"),
        P("tp"),
        P("ep", None, "tp", None),
        P("ep", None, "tp", None),
        P("ep"),
        P("tp", "ep"),
        P("tp"),
        P("ep"),
        P(),
        P(),
        P("ep", None, "tp"),
        P("ep", None, "tp"),
        P("ep", "tp", None),
        P("ep", "tp"),
        P("ep", "tp"),
        P("tp", "ep"),
        P("ep"),
    )
    out_specs = (P(None, "ep"), P("ep", "tp"), P("ep", "tp"))
    return jax.shard_map(
        per_device, mesh=mesh, in_specs=in_specs, out_specs=out_specs, check_vma=False
    )
```

profile of v0, /device:TPU:0, one launch (start us, length us, event | category | flops | bytes accessed | tf_op | source)
XLA Modules:
  0.0 456.8 jit_solution(16024287437481387308)
XLA Ops:
  7.3 1.1 fusion.35
  8.4 23.1 %psum.28 = f32[128]{0:T(128)S(1)} all-reduce(f32[128]{0:T(128)S(1)} %fusion.35), channel_id=1, replica_groups=mesh['ep'=8,'tp'=4] {'ep'}, use_global_device_ids=true, to_apply=%region_1.0 | all-reduce | flops 128 | bytes 1024 | tf_op jit(solution)/shard_map/psum | solution.py:10
  31.5 2.3 convolution_convert_fusion.2
  34.5 0.6 reduce-window.16
  35.0 0.2 slice_reduce_fusion
  35.7 1.4 scatter_custom_fusion
  37.2 56.6 %reduce-scatter.4.cloned.1.call-done = bf16[16,1024]{1,0:T(8,128)(2,1)} async-done(((bf16[128,1024]{1,0:T(8,128)(2,1)}), bf16[16,1024]{1,0:T(8,128)(2,1)}) %reduce-scatter.4.cloned.1.call-update) | async-done | bytes 32784 | tf_op jit(solution)/shard_map/reduce_scatter | solution.py:15
  93.8 0.7 slice.43
  94.5 5.7 %fusion.42 = (f32[16,2,2,1024]{3,2,1,0:T(2,128)S(1)}, f32[16,2,2,1024]{3,2,1,0:T(2,128)S(1)}) fusion(pred[16,1024]{1,0:T(8,128)(4,1)S(1)} %iota_compare_fusion, f32[2,2]{1,0:T(2,128)S(1)} %add.104, bf16[16,2,2,128]{3,2,1,0:T(2,128)(2,1)S(1)} %reshape.137, bf16[16,1024,2,128]{3,2,1,0:T(2,128)(2,1)} %param.27), kind=kOutput, calls=%fused_computation.45 | convolution fusion | flops 17432576 | bytes 8945680 | tf_op jit(solution)/shard_map/skgd,slkd->skgl/dot_general | solution.py:95
  100.2 0.2 reshape.138
  100.4 79.2 %reduce-window.14 = f32[16,2,2,8,128]{4,3,2,1,0:T(8,128)S(1)} reduce-window(f32[16,2,2,8,128]{4,3,2,1,0:T(8,128)S(1)} %reshape.138, f32[]{:T(128)} %constant.27.clone.1), window={size=1x1x1x1x128 pad=0_0x0_0x0_0x0_0x0_127}, to_apply=%region_3.4 | reduce-window | flops 8323072 | bytes 524292 | tf_op jit(solution)/shard_map/reduce-window
  179.7 0.3 copy.78
  180.4 5.9 %multiply_reduce_fusion.2 = (f32[16,2,2]{2,1,0:T(2,128)S(1)}, f32[16,2,2,128]{3,2,1,0:T(2,128)S(1)}) fusion(bf16[16,1024,2,128]{3,2,1,0:T(2,128)(2,1)} %param.28, pred[16,1024]{1,0:T(8,128)(4,1)S(1)} %iota_compare_fusion, f32[16,2,2,1024]{3,2,1,0:T(2,128)S(1)} %reduce_window_sum.30, f32[16,2,2,1024]{3,2,1,0:T(2,128)S(1)} %get-tuple-element.6), kind=kOutput, calls=%fused_computation.65 | convolution fusion | flops 18104256 | bytes 8962304 | tf_op jit(solution)/shard_map/skgl,slkd->skgd/dot_general | solution.py:107
  186.7 30.6 %all_gather.12 = bf16[128,512]{1,0:T(8,128)(2,1)S(1)} all-gather(bf16[16,512]{1,0:T(8,128)(2,1)S(1)} %reshape.140), channel_id=1, replica_groups=mesh['ep'=8,'tp'=4] {'ep'}, dimensions={0}, use_global_device_ids=true | all-gather | bytes 147456 | tf_op jit(solution)/shard_map/all_gather | solution.py:25
  217.2 0.9 convolution_convert_fusion.3
  218.2 31.0 %all-reduce.4.cloned.1.call-done = bf16[128,512]{1,0:T(8,128)(2,1)} async-done(((bf16[128,512]{1,0:T(8,128)(2,1)}), bf16[128,512]{1,0:T(8,128)(2,1)}) %all-reduce.4.cloned.1.call-update) | async-done | bytes 131088 | tf_op jit(solution)/shard_map/psum | solution.py:29
  249.1 1.0 multiply_reduce_fusion.1
  250.1 21.3 %psum.30 = f32[128]{0:T(128)S(1)} all-reduce(f32[128]{0:T(128)S(1)} %multiply_reduce_fusion.1), channel_id=1, replica_groups=mesh['ep'=8,'tp'=4] {'ep'}, use_global_device_ids=true, to_apply=%region_8.9 | all-reduce | flops 128 | bytes 1024 | tf_op jit(solution)/shard_map/psum | solution.py:10
  271.5 1.0 multiply_convert_fusion
  272.5 2.0 gather_fusion
  274.5 0.7 constant_dynamic-slice_fusion
  275.2 3.4 all-to-all-start
  278.6 2.8 convolution_convert_fusion.1
  281.5 4.4 all-to-all-done
  285.9 6.7 %all_gather.13 = bf16[1,64,4096]{2,1,0:T(8,128)(2,1)S(1)} all-gather(bf16[1,16,4096]{2,1,0:T(8,128)(2,1)S(1)} %bitcast.68), channel_id=1, replica_groups=mesh['ep'=8,'tp'=4] {'tp'}, dimensions={1}, use_global_device_ids=true | all-gather | bytes 655360 | tf_op jit(solution)/shard_map/all_gather | solution.py:132
  292.5 2.1 fusion.11
  294.6 3.8 fusion.4
  298.5 0.7 copy.91
  299.3 0.6 fusion.64
  299.9 46.4 %reduce-scatter.8.cloned.1.call-done = bf16[16,2048]{1,0:T(8,128)(2,1)} async-done(((bf16[128,2048]{1,0:T(8,128)(2,1)}), bf16[16,2048]{1,0:T(8,128)(2,1)}) %reduce-scatter.8.cloned.1.call-update) | async-done | bytes 65552 | tf_op jit(solution)/shard_map/reduce_scatter | solution.py:15
  346.2 0.8 convert_element_type.85
  347.1 30.8 %all_gather.15 = bf16[128,1024]{1,0:T(8,128)(2,1)S(1)} all-gather(bf16[16,1024]{1,0:T(8,128)(2,1)S(1)} %fusion.47), channel_id=1, replica_groups=mesh['ep'=8,'tp'=4] {'ep'}, dimensions={0}, use_global_device_ids=true | all-gather | bytes 294912 | tf_op jit(solution)/shard_map/all_gather | solution.py:25
  378.0 4.9 %copy.87 = bf16[1,16,4096]{1,0,2:T(2,128)(2,1)} copy(bf16[1,16,4096]{2,1,0:T(8,128)(2,1)} %reduce-scatter.6.cloned.1.call-done) | data formatting | bytes 262144 | tf_op jit(solution)/shard_map/reduce_scatter | solution.py:134
  382.9 0.5 broadcast.126
  383.4 23.4 %reduce.2 = bf16[4096,16]{1,0:T(8,128)(2,1)S(1)} reduce(bf16[4096,1,16]{2,1,0:T(2,128)(2,1)} %bitcast.64, bf16[]{:T(256)} %broadcast.126), dimensions={1}, to_apply=%bitcast.53.reduce_sub_computation | reduce | bytes 262146
  406.8 1.7 reshape.179
  408.5 3.4 all-to-all-start.1
  412.0 2.2 convolution_convert_fusion.4
  414.2 5.1 %all-to-all-done.1 = bf16[8,2,4096]{2,1,0:T(2,128)(2,1)S(1)} async-done(((bf16[8,2,4096]{2,1,0:T(2,128)(2,1)}), bf16[8,2,4096]{2,1,0:T(2,128)(2,1)S(1)}, u32[]{:S(2)}, u32[]{:S(2)}) %all-to-all-start.1) | async-done | bytes 131104 | tf_op jit(solution)/shard_map/all_to_all | solution.py:137
  419.3 3.9 reshape.180
  423.2 4.4 copy.88
  427.7 7.2 %all-gather = bf16[8,1,64,512]{3,0,1,2:T(8,128)(2,1)S(1)} all-gather(bf16[8,1,16,512]{3,0,1,2:T(8,128)(2,1)S(1)} %bitcast_bitcast_fusion), channel_id=2, replica_groups=mesh['ep'=8,'tp'=4] {'tp'}, dimensions={2}, use_global_device_ids=true | all-gather | bytes 655360 | tf_op jit(solution)/shard_map/all_gather | solution.py:138
  434.8 0.2 copy.90
  435.0 1.2 gather_fusion.1
  436.2 0.3 reshape.148
  436.5 0.7 multiply_reduce_fusion
  437.2 11.4 %all-reduce.6.cloned.1.call-done = bf16[128,512]{1,0:T(8,128)(2,1)} async-done(((bf16[128,512]{1,0:T(8,128)(2,1)}), bf16[128,512]{1,0:T(8,128)(2,1)}) %all-reduce.6.cloned.1.call-update) | async-done | bytes 131088 | tf_op jit(solution)/shard_map/psum | solution.py:29
  448.6 1.6 add_convert_fusion
  (74 shorter events, 2.2 us)
Async XLA Ops:
  7.2 287.4 %copy-start = (bf16[1,256,4096]{2,1,0:T(8,128)(2,1)S(1)}, bf16[1,256,4096]{2,1,0:T(8,128)(2,1)}, u32[]{:S(2)}) copy-start(bf16[1,256,4096]{2,1,0:T(8,128)(2,1)} %param.37) | copy-start | bytes 6291460
  7.2 26.8 %copy-start.6 = (s32[128,2]{0,1:T(2,128)S(1)}, s32[128,2]{0,1:T(2,128)}, u32[]{:S(2)}) copy-start(s32[128,2]{0,1:T(2,128)} %param.33) | copy-start | bytes 3076
  7.2 27.2 %copy-start.12 = (f32[4]{0:T(128)S(1)}, f32[4]{0:T(128)}, u32[]{:S(2)}) copy-start(f32[4]{0:T(128)} %param.26) | copy-start | bytes 52
  7.2 29.9 %copy-start.11 = (s32[16]{0:T(128)S(1)}, s32[16]{0:T(128)}, u32[]{:S(2)}) copy-start(s32[16]{0:T(128)} %param.29) | copy-start | bytes 196
  7.2 86.6 %reduce-scatter.4.cloned.1.call-start = ((), (), s32[]{:S(2)}) async-start(), calls=%async_computation.5 | async-start | bytes 294912 | tf_op jit(solution)/shard_map/reduce_scatter | solution.py:15
  33.9 215.2 %all-reduce.4.cloned.1.call-start = ((), (), s32[]{:S(2)}) async-start(), calls=%async_computation.6 | async-start | bytes 262144 | tf_op jit(solution)/shard_map/psum | solution.py:29
  180.4 6.1 %copy-start.10 = (f32[512]{0:T(512)S(1)}, f32[512]{0:T(512)}, u32[]{:S(2)}) copy-start(f32[512]{0:T(512)} %param.31) | copy-start | bytes 6148
  180.4 36.8 %copy-start.3 = (bf16[512,512]{1,0:T(8,128)(2,1)S(1)}, bf16[512,512]{1,0:T(8,128)(2,1)}, u32[]{:S(2)}) copy-start(bf16[512,512]{1,0:T(8,128)(2,1)} %param.30) | copy-start | bytes 1572868
  180.4 68.7 %copy-start.1 = (bf16[128,512]{1,0:T(8,128)(2,1)S(1)}, bf16[128,512]{1,0:T(8,128)(2,1)}, u32[]{:S(2)}) copy-start(bf16[128,512]{1,0:T(8,128)(2,1)} %param.21) | copy-start | bytes 393220
  180.4 91.1 %copy-start.8 = (f32[512]{0:T(512)S(1)}, f32[512]{0:T(512)}, u32[]{:S(2)}) copy-start(f32[512]{0:T(512)} %param.32) | copy-start | bytes 6148
  275.2 10.7 %all-to-all-start = ((bf16[8,16,512]{2,1,0:T(8,128)(2,1)}), bf16[8,16,512]{2,1,0:T(8,128)(2,1)S(1)}, u32[]{:S(2)}, u32[]{:S(2)}) async-start(bf16[8,16,512]{2,1,0:T(8,128)(2,1)} %constant_dynamic-slice_fusion), calls=%async_computation.1 | async-start | bytes 262144 | tf_op jit(solution)/shard_map/all_to_all | solution.py:131
  278.6 67.7 %reduce-scatter.8.cloned.1.call-start = ((), (), s32[]{:S(2)}) async-start(), calls=%async_computation.8 | async-start | bytes 589824 | tf_op jit(solution)/shard_map/reduce_scatter | solution.py:15
  281.4 96.5 %reduce-scatter.6.cloned.1.call-start = ((), (), s32[]{:S(2)}) async-start(), calls=%async_computation.7 | async-start | bytes 655360 | tf_op jit(solution)/shard_map/reduce_scatter | solution.py:134
  294.6 3.9 copy-start.7
  294.6 4.6 %copy-start.5 = (bf16[16,1024]{1,0:T(8,128)(2,1)S(1)}, bf16[16,1024]{1,0:T(8,128)(2,1)}, u32[]{:S(2)}) copy-start(bf16[16,1024]{1,0:T(8,128)(2,1)} %reduce-scatter.4.cloned.1.call-done) | copy-start | bytes 98308
  408.5 10.7 %all-to-all-start.1 = ((bf16[8,2,4096]{2,1,0:T(2,128)(2,1)}), bf16[8,2,4096]{2,1,0:T(2,128)(2,1)S(1)}, u32[]{:S(2)}, u32[]{:S(2)}) async-start(bf16[8,2,4096]{2,1,0:T(2,128)(2,1)} %reshape.179), calls=%async_computation.3 | async-start | bytes 262144 | tf_op jit(solution)/shard_map/all_to_all | solution.py:137
  411.9 36.7 %all-reduce.6.cloned.1.call-start = ((), (), s32[]{:S(2)}) async-start(), calls=%async_computation.9 | async-start | bytes 262144 | tf_op jit(solution)/shard_map/psum | solution.py:29
  434.8 1.7 copy-start.4
  435.0 13.6 %copy-start.2 = (bf16[128,512]{1,0:T(8,128)(2,1)S(1)}, bf16[128,512]{1,0:T(8,128)(2,1)}, u32[]{:S(2)}) copy-start(bf16[128,512]{1,0:T(8,128)(2,1)} %all-reduce.4.cloned.1.call-done) | copy-start | bytes 393220
  435.0 13.6 %copy-start.9 = (f32[512]{0:T(512)S(1)}, f32[512]{0:T(512)}, u32[]{:S(2)}) copy-start(f32[512]{0:T(512)} %param.41) | copy-start | bytes 6148
Sparse Core Ops, SparseCore 0:
  34.0 59.7 reduce-scatter.3
  218.3 30.8 all-reduce.3
  282.7 63.4 reduce-scatter.7
  348.6 20.6 reduce-scatter.5
  415.3 33.2 all-reduce.5
where the time goes:
time: 458 us; the launch traced here: 457 us
  waiting for transfers between devices  155 us (34%)
  blocking collectives  120 us (26%)
  other arithmetic  110 us (24%)
  matrix products  25.7 us (6%)
  local copies, waits for them, and re-layouts  25.2 us (6%)
  between operations  14.2 us (3%)
  starting transfers between devices  6.96 us (2%)
    reduce_scatter x2, waiting for transfers between devices, to_heads(): lax.psum_scatter(jnp.dot(normed, weights, preferred_element_type=jnp.floa...  103 us
    another operation x4, other arithmetic  79.9 us
    all_gather x2, blocking collectives, from_heads(): lax.all_gather(values, 'ep', axis=0, tiled=True)  61.4 us
    psum x2, blocking collectives, rms_scale(): squares = lax.psum(jnp.sum(values * values, axis=1), 'ep')  44.5 us
    psum x2, waiting for transfers between devices, from_heads(): return lax.psum(partial_value.astype(jnp.bfloat16), 'tp')  42.3 us
    unnamed x1, other arithmetic  23.4 us
  transfers between devices with their start and end apart: 7, of which 6 were waited for; matrix products, arithmetic and copies ran while one was open for 6% of the time, Pallas kernels for 0%

commit v1 on v0

--- a/solution.py
+++ b/solution.py
@@ -26,7 +26,7 @@
         weights,
         preferred_element_type=jnp.float32,
     )
-    return lax.psum(partial_value.astype(jnp.bfloat16), "tp")
+    return jnp.sum(lax.all_gather(partial_value.astype(jnp.bfloat16), "tp"), axis=0)
 
 
 def expert_terms(inputs, gate_w, up_w, down_w):

time: 458 us -> 421 us (0.919)
  waiting for transfers between devices: 155 us -> 108 us
  blocking collectives: 120 us -> 134 us
    psum x2 -> x0, waiting for transfers between devices: 42.3 us -> none  [from_heads(): return lax.psum(partial_value.astype(jnp.bfloat16), 'tp')]
    all_gather x0 -> x2, blocking collectives: none -> 14.3 us  [from_heads(): lax.all_gather(partial_value.astype(jnp.bfloat16), 'tp')]
    all_to_all x1, waiting for transfers between devices: 5.08 us -> 0.01 us  [per_device(): lax.all_to_all(summed, 'ep', split_axis=2, concat_axis=0, tiled=True)]
  transfers between devices with their start and end apart: 7 -> 5, of which waited for: 6 -> 3; matrix products, arithmetic and copies ran while one was open for 6% -> 4% of each run, Pallas kernels for 0% -> 0%
where the time goes in v1:
time: 421 us; the launch traced here: 420 us
  blocking collectives  134 us (32%)
  other arithmetic  108 us (26%)
  waiting for transfers between devices  108 us (26%)
  local copies, waits for them, and re-layouts  24.6 us (6%)
  matrix products  24.4 us (6%)
  between operations  14.2 us (3%)
  starting transfers between devices  7 us (2%)
    reduce_scatter x2, waiting for transfers between devices, to_heads(): lax.psum_scatter(jnp.dot(normed, weights, preferred_element_type=jnp.floa...  103 us
    another operation x4, other arithmetic  79.9 us
    all_gather x2, blocking collectives, from_heads(): lax.all_gather(values, 'ep', axis=0, tiled=True)  63.3 us
    psum x2, blocking collectives, rms_scale(): squares = lax.psum(jnp.sum(values * values, axis=1), 'ep')  42.6 us
    unnamed x1, other arithmetic  23.4 us
    all_gather x2, blocking collectives, from_heads(): lax.all_gather(partial_value.astype(jnp.bfloat16), 'tp')  14.3 us
  transfers between devices with their start and end apart: 5, of which 3 were waited for; matrix products, arithmetic and copies ran while one was open for 4% of the time, Pallas kernels for 0%

profile of v1, /device:TPU:0, one launch (start us, length us, event | category | flops | bytes accessed | tf_op | source)
XLA Modules:
  0.0 419.9 jit_solution(10838322985246634183)
XLA Ops:
  7.3 1.1 fusion.35
  8.4 23.1 %psum.14 = f32[128]{0:T(128)S(1)} all-reduce(f32[128]{0:T(128)S(1)} %fusion.35), channel_id=1, replica_groups=mesh['ep'=8,'tp'=4] {'ep'}, use_global_device_ids=true, to_apply=%region_1.0 | all-reduce | flops 128 | bytes 1024 | tf_op jit(solution)/shard_map/psum | solution.py:10
  31.5 2.3 convolution_convert_fusion.2
  34.0 0.1 eq.29
  34.2 0.1 eq.25
  34.4 0.6 reduce-window.16
  35.0 0.2 slice_reduce_fusion
  35.4 0.1 mul.139
  35.6 1.4 scatter_custom_fusion
  37.1 56.7 %reduce-scatter.4.cloned.1.call-done = bf16[16,1024]{1,0:T(8,128)(2,1)} async-done(((bf16[128,1024]{1,0:T(8,128)(2,1)}), bf16[16,1024]{1,0:T(8,128)(2,1)}) %reduce-scatter.4.cloned.1.call-update) | async-done | bytes 32784 | tf_op jit(solution)/shard_map/reduce_scatter | solution.py:15
  93.8 0.7 slice.43
  94.5 5.7 %fusion.42 = (f32[16,2,2,1024]{3,2,1,0:T(2,128)S(1)}, f32[16,2,2,1024]{3,2,1,0:T(2,128)S(1)}) fusion(pred[16,1024]{1,0:T(8,128)(4,1)S(1)} %iota_compare_fusion, f32[2,2]{1,0:T(2,128)S(1)} %add.100, bf16[16,2,2,128]{3,2,1,0:T(2,128)(2,1)S(1)} %reshape.137, bf16[16,1024,2,128]{3,2,1,0:T(2,128)(2,1)} %param.27), kind=kOutput, calls=%fused_computation.45 | convolution fusion | flops 17432576 | bytes 8945680 | tf_op jit(solution)/shard_map/skgd,slkd->skgl/dot_general | solution.py:95
  100.2 0.2 reshape.138
  100.4 79.2 %reduce-window.14 = f32[16,2,2,8,128]{4,3,2,1,0:T(8,128)S(1)} reduce-window(f32[16,2,2,8,128]{4,3,2,1,0:T(8,128)S(1)} %reshape.138, f32[]{:T(128)} %constant.31.clone.1), window={size=1x1x1x1x128 pad=0_0x0_0x0_0x0_0x0_127}, to_apply=%region_3.4 | reduce-window | flops 8323072 | bytes 524292 | tf_op jit(solution)/shard_map/reduce-window
  179.7 0.3 copy.78
  180.2 0.1 reduce_window_sum.30
  180.4 5.9 %multiply_reduce_fusion.2 = (f32[16,2,2]{2,1,0:T(2,128)S(1)}, f32[16,2,2,128]{3,2,1,0:T(2,128)S(1)}) fusion(bf16[16,1024,2,128]{3,2,1,0:T(2,128)(2,1)} %param.28, pred[16,1024]{1,0:T(8,128)(4,1)S(1)} %iota_compare_fusion, f32[16,2,2,1024]{3,2,1,0:T(2,128)S(1)} %reduce_window_sum.30, f32[16,2,2,1024]{3,2,1,0:T(2,128)S(1)} %get-tuple-element.6), kind=kOutput, calls=%fused_computation.65 | convolution fusion | flops 18104256 | bytes 8962304 | tf_op jit(solution)/shard_map/skgl,slkd->skgd/dot_general | solution.py:107
  186.7 30.6 %all_gather.24 = bf16[128,512]{1,0:T(8,128)(2,1)S(1)} all-gather(bf16[16,512]{1,0:T(8,128)(2,1)S(1)} %reshape.140), channel_id=1, replica_groups=mesh['ep'=8,'tp'=4] {'ep'}, dimensions={0}, use_global_device_ids=true | all-gather | bytes 147456 | tf_op jit(solution)/shard_map/all_gather | solution.py:25
  217.2 0.2 convolution_convert_fusion.3
  217.5 7.2 %all-gather = bf16[512,512]{1,0:T(8,128)(2,1)S(1)} all-gather(bf16[128,512]{1,0:T(8,128)(2,1)S(1)} %convolution_convert_fusion.3), channel_id=2, replica_groups=mesh['ep'=8,'tp'=4] {'tp'}, dimensions={0}, use_global_device_ids=true | all-gather | bytes 655360 | tf_op jit(solution)/shard_map/all_gather | solution.py:29
  224.8 19.5 %psum.15 = f32[128]{0:T(128)S(1)} all-reduce(f32[128]{0:T(128)S(1)} %multiply_reduce_fusion.1), channel_id=1, replica_groups=mesh['ep'=8,'tp'=4] {'ep'}, use_global_device_ids=true, to_apply=%region_8.9 | all-reduce | flops 128 | bytes 1024 | tf_op jit(solution)/shard_map/psum | solution.py:10
  244.4 2.0 gather_fusion
  246.4 0.7 constant_dynamic-slice_fusion
  247.1 3.4 all-to-all-start
  250.5 2.8 convolution_convert_fusion.1
  253.4 4.4 %all-to-all-done = bf16[8,16,512]{2,1,0:T(8,128)(2,1)S(1)} async-done(((bf16[8,16,512]{2,1,0:T(8,128)(2,1)}), bf16[8,16,512]{2,1,0:T(8,128)(2,1)S(1)}, u32[]{:S(2)}, u32[]{:S(2)}) %all-to-all-start) | async-done | bytes 131104 | tf_op jit(solution)/shard_map/all_to_all | solution.py:131
  257.8 6.7 %all_gather.27 = bf16[1,64,4096]{2,1,0:T(8,128)(2,1)S(1)} all-gather(bf16[1,16,4096]{2,1,0:T(8,128)(2,1)S(1)} %bitcast.72), channel_id=1, replica_groups=mesh['ep'=8,'tp'=4] {'tp'}, dimensions={1}, use_global_device_ids=true | all-gather | bytes 655360 | tf_op jit(solution)/shard_map/all_gather | solution.py:132
  264.5 2.0 fusion.11
  266.5 3.8 fusion.4
  270.6 0.6 fusion.64
  271.2 46.8 %reduce-scatter.8.cloned.1.call-done = bf16[16,2048]{1,0:T(8,128)(2,1)} async-done(((bf16[128,2048]{1,0:T(8,128)(2,1)}), bf16[16,2048]{1,0:T(8,128)(2,1)}) %reduce-scatter.8.cloned.1.call-update) | async-done | bytes 65552 | tf_op jit(solution)/shard_map/reduce_scatter | solution.py:15
  318.0 0.8 convert_element_type.89
  318.9 32.7 %all_gather.29 = bf16[128,1024]{1,0:T(8,128)(2,1)} all-gather(bf16[16,1024]{1,0:T(8,128)(2,1)S(1)} %fusion.47), channel_id=1, replica_groups=mesh['ep'=8,'tp'=4] {'ep'}, dimensions={0}, use_global_device_ids=true | all-gather | bytes 294912 | tf_op jit(solution)/shard_map/all_gather | solution.py:25
  351.6 4.9 %copy.87 = bf16[1,16,4096]{1,0,2:T(2,128)(2,1)} copy(bf16[1,16,4096]{2,1,0:T(8,128)(2,1)} %reduce-scatter.6.cloned.1.call-done) | data formatting | bytes 262144 | tf_op jit(solution)/shard_map/reduce_scatter | solution.py:134
  356.5 0.5 broadcast.126
  357.0 23.4 %reduce.4 = bf16[4096,16]{1,0:T(8,128)(2,1)S(1)} reduce(bf16[4096,1,16]{2,1,0:T(2,128)(2,1)} %bitcast.66, bf16[]{:T(256)} %broadcast.126), dimensions={1}, to_apply=%bitcast.55.reduce_sub_computation | reduce | bytes 262146
  380.5 1.7 reshape.181
  382.2 3.5 all-to-all-start.1
  385.7 1.6 convolution_convert_fusion.4
  387.3 7.1 %all-gather.2 = bf16[512,512]{1,0:T(8,128)(2,1)S(1)} all-gather(bf16[128,512]{1,0:T(8,128)(2,1)S(1)} %convolution_convert_fusion.4), channel_id=4, replica_groups=mesh['ep'=8,'tp'=4] {'tp'}, dimensions={0}, use_global_device_ids=true | all-gather | bytes 655360 | tf_op jit(solution)/shard_map/all_gather | solution.py:29
  394.6 4.0 reshape.182
  398.5 4.4 %copy.88 = bf16[1,16,4096]{2,1,0:T(8,128)(2,1)S(1)} copy(bf16[1,16,4096]{1,0,2:T(2,128)(2,1)} %bitcast.67) | data formatting | bytes 262144 | tf_op jit(solution)/shard_map/all_to_all | solution.py:137
  403.0 7.3 %all-gather.1 = bf16[8,1,64,512]{3,0,1,2:T(8,128)(2,1)S(1)} all-gather(bf16[8,1,16,512]{3,0,1,2:T(8,128)(2,1)S(1)} %bitcast_bitcast_fusion), channel_id=3, replica_groups=mesh['ep'=8,'tp'=4] {'tp'}, dimensions={2}, use_global_device_ids=true | all-gather | bytes 655360 | tf_op jit(solution)/shard_map/all_gather | solution.py:138
  410.3 0.2 copy.90
  410.5 1.2 gather_fusion.1
  411.6 0.3 reshape.148
  412.0 0.7 multiply_reduce_fusion
  412.7 0.7 add_convert_fusion
  (68 shorter events, 2.0 us)
Async XLA Ops:
  7.2 259.4 %copy-start = (bf16[1,256,4096]{2,1,0:T(8,128)(2,1)S(1)}, bf16[1,256,4096]{2,1,0:T(8,128)(2,1)}, u32[]{:S(2)}) copy-start(bf16[1,256,4096]{2,1,0:T(8,128)(2,1)} %param.37) | copy-start | bytes 6291460
  7.2 26.7 %copy-start.4 = (s32[128,2]{0,1:T(2,128)S(1)}, s32[128,2]{0,1:T(2,128)}, u32[]{:S(2)}) copy-start(s32[128,2]{0,1:T(2,128)} %param.33) | copy-start | bytes 3076
  7.2 27.1 %copy-start.10 = (f32[4]{0:T(128)S(1)}, f32[4]{0:T(128)}, u32[]{:S(2)}) copy-start(f32[4]{0:T(128)} %param.26) | copy-start | bytes 52
  7.2 29.9 %copy-start.9 = (s32[16]{0:T(128)S(1)}, s32[16]{0:T(128)}, u32[]{:S(2)}) copy-start(s32[16]{0:T(128)} %param.29) | copy-start | bytes 196
  7.2 86.6 %reduce-scatter.4.cloned.1.call-start = ((), (), s32[]{:S(2)}) async-start(), calls=%async_computation.5 | async-start | bytes 294912 | tf_op jit(solution)/shard_map/reduce_scatter | solution.py:15
  180.4 6.1 %copy-start.8 = (f32[512]{0:T(512)S(1)}, f32[512]{0:T(512)}, u32[]{:S(2)}) copy-start(f32[512]{0:T(512)} %param.31) | copy-start | bytes 6148
  180.4 36.8 %copy-start.2 = (bf16[512,512]{1,0:T(8,128)(2,1)S(1)}, bf16[512,512]{1,0:T(8,128)(2,1)}, u32[]{:S(2)}) copy-start(bf16[512,512]{1,0:T(8,128)(2,1)} %param.30) | copy-start | bytes 1572868
  186.3 38.4 %copy-start.1 = (bf16[128,512]{1,0:T(8,128)(2,1)S(1)}, bf16[128,512]{1,0:T(8,128)(2,1)}, u32[]{:S(2)}) copy-start(bf16[128,512]{1,0:T(8,128)(2,1)} %param.21) | copy-start | bytes 393220
  186.3 58.0 %copy-start.6 = (f32[512]{0:T(512)S(1)}, f32[512]{0:T(512)}, u32[]{:S(2)}) copy-start(f32[512]{0:T(512)} %param.32) | copy-start | bytes 6148
  247.1 10.7 %all-to-all-start = ((bf16[8,16,512]{2,1,0:T(8,128)(2,1)}), bf16[8,16,512]{2,1,0:T(8,128)(2,1)S(1)}, u32[]{:S(2)}, u32[]{:S(2)}) async-start(bf16[8,16,512]{2,1,0:T(8,128)(2,1)} %constant_dynamic-slice_fusion), calls=%async_computation.1 | async-start | bytes 262144 | tf_op jit(solution)/shard_map/all_to_all | solution.py:131
  250.5 67.5 %reduce-scatter.8.cloned.1.call-start = ((), (), s32[]{:S(2)}) async-start(), calls=%async_computation.7 | async-start | bytes 589824 | tf_op jit(solution)/shard_map/reduce_scatter | solution.py:15
  253.4 98.3 %reduce-scatter.6.cloned.1.call-start = ((), (), s32[]{:S(2)}) async-start(), calls=%async_computation.6 | async-start | bytes 655360 | tf_op jit(solution)/shard_map/reduce_scatter | solution.py:134
  266.5 3.9 copy-start.5
  266.5 4.0 copy-start.3
  382.2 12.4 %all-to-all-start.1 = ((bf16[8,2,4096]{2,1,0:T(2,128)(2,1)}), bf16[8,2,4096]{2,1,0:T(2,128)(2,1)S(1)}, u32[]{:S(2)}, u32[]{:S(2)}) async-start(bf16[8,2,4096]{2,1,0:T(2,128)(2,1)} %reshape.181), calls=%async_computation.3 | async-start | bytes 262144 | tf_op jit(solution)/shard_map/all_to_all | solution.py:137
  410.5 2.2 copy-start.7
Sparse Core Ops, SparseCore 0:
  34.0 59.7 reduce-scatter.3
  254.6 63.3 reduce-scatter.7
  320.5 20.6 reduce-scatter.5
